TPU v7x, 768 devices: a whole 4x8x12 slice. The times are simulated.
768 devices in a mesh: ep: 48 (over z, x), tp: 16 (over y, core).
Axes of the slice: x: 4, y: 8, z: 12, core: 2. Of those that a mesh axis runs over, the one named last changes fastest.
Arguments:
- tokens: bfloat16 [6144, 2048], P('ep'), may hold values from -6 to 6
- chosen: int32 [48, 48, 7], P('ep'), may hold values from -1 to 127, as said below
- pick_weight: float32 [48, 48, 7], P('ep'), may hold values from 0.2 to 1
- gate_weight: bfloat16 [48, 2048, 4096], P('ep', None, 'tp'), may hold values from -0.125 to 0.125
- up_weight: bfloat16 [48, 2048, 4096], P('ep', None, 'tp'), may hold values from -0.125 to 0.125
- down_weight: bfloat16 [48, 4096, 2048], P('ep', 'tp'), may hold values from -0.09375 to 0.09375
Outputs:
- combined: bfloat16 [6144, 2048], P('ep', 'tp')
Inputs may be any that keep to these rules, and one draw needn't show every extreme that they name: `chosen`: within one group and one expert the named positions are distinct, and the filled slots come first. From each group every expert takes at least 3 tokens and at most 7; every expert takes exactly 7 tokens from some group, and exactly 240 tokens in all.
All inputs are finite; a program needn't handle non-finite values.
Results may differ from a plain program's by a relative error of at most 0.019.
Values may be sent and summed in bfloat16 or wider, within the bound.
A program may use at most 64 MiB of HBM per device.

v0:
```python
import jax
import jax.numpy as jnp
from jax import lax
from jax.sharding import PartitionSpec as P


def laid_out(parts, dim):
    parts = jnp.moveaxis(parts, 0, dim)
    dims = parts.shape
    return parts.reshape(*dims[:dim], dims[dim] * dims[dim + 1], *dims[dim + 2 :])


def copy_for_each(x, axis):
    count = lax.axis_size(axis)
    return lax.all_to_all(jnp.broadcast_to(x[None], (count, *x.shape)), axis, 0, 0, tiled=True)


def gather_directly(x, axis, dim):
    return laid_out(copy_for_each(x, axis), dim)


def in_blocks(x, dim, count):
    before, after = (x.shape[:dim], x.shape[dim + 1 :])
    return jnp.moveaxis(x.reshape(*before, count, -1, *after), dim, 0)


def summed_on_arrival(x, axis, dim):
    count = lax.axis_size(axis)
    parts = lax.all_to_all(in_blocks(x, dim, count), axis, 0, 0, tiled=True)
    return jnp.sum(parts.astype(jnp.float32), axis=0)


def on_device(tokens, chosen, pick_weight, gate_weight, up_weight, down_weight):
    model_width = tokens.shape[1]
    experts = chosen.shape[1]
    slot_count = chosen.shape[2]
    chosen_ids = chosen[0]
    filled = chosen_ids >= 0
    safe_ids = jnp.where(filled, chosen_ids, 0).reshape(-1)
    picked = jnp.take(tokens, safe_ids, axis=0)
    picked = jnp.where(filled.reshape(-1, 1), picked, jnp.zeros((), tokens.dtype))
    picked = picked.reshape(experts, slot_count, model_width)
    col_width = model_width // lax.axis_size("tp")
    tp_rank = lax.axis_index("tp")
    col_slice = lax.dynamic_slice_in_dim(picked, tp_rank * col_width, col_width, 2)
    arrived = lax.all_to_all(col_slice, "ep", split_axis=0, concat_axis=0, tiled=True)
    received = gather_directly(arrived, "tp", 2)
    expert_rows = received.reshape(-1, model_width)
    gate_pre = jnp.dot(expert_rows, gate_weight[0], preferred_element_type=jnp.float32)
    up_pre = jnp.dot(expert_rows, up_weight[0], preferred_element_type=jnp.float32)
    hidden = (jax.nn.silu(gate_pre) * up_pre).astype(jnp.bfloat16)
    down_local = down_weight[0]
    summed = summed_on_arrival(
        jnp.einsum("fd,rf->dr", down_local, hidden, preferred_element_type=jnp.float32).astype(
            jnp.bfloat16
        ),
        "tp",
        0,
    ).astype(jnp.bfloat16)
    returned = lax.all_to_all(summed, "ep", split_axis=1, concat_axis=1, tiled=True)
    weights = jnp.where(filled, pick_weight[0], jnp.zeros((), jnp.float32)).reshape(-1)
    positions = lax.iota(jnp.int32, tokens.shape[0])
    onehot = jnp.where(
        positions[:, None] == safe_ids[None, :], weights[None, :], jnp.zeros((), jnp.float32)
    )
    combined = jnp.einsum(
        "tk,wk->tw",
        onehot,
        returned.astype(jnp.float32),
        precision=lax.Precision.HIGHEST,
        preferred_element_type=jnp.float32,
    )
    return combined.astype(jnp.bfloat16)


def solution(mesh):
    return jax.shard_map(
        on_device,
        mesh=mesh,
        in_specs=(
            P("ep", None),
            P("ep", None, None),
            P("ep", None, None),
            P("ep", None, "tp"),
            P("ep", None, "tp"),
            P("ep", "tp", None),
        ),
        out_specs=P("ep", "tp"),
        check_vma=False,
    )
```

profile of v0, /device:TPU:1, one launch (start us, length us, event | category | flops | bytes accessed | tf_op | source)
XLA Modules:
  0.0 150.4 jit_solution(8034597544847844044)
XLA Ops:
  0.0 0.0 copy-start
  0.0 0.8 compare_and_fusion
  0.8 0.8 copy.21
  1.6 0.1 copy.24
  1.7 0.1 copy.23
  1.8 0.1 squeeze.22
  1.9 5.5 %gather_fusion = bf16[336,2048]{1,0:T(8,128)(2,1)S(1)} fusion(bf16[128,2048]{1,0:T(8,128)(2,1)} %param.6, s32[1024]{0:T(1024)S(1)} %pad_clamp_fusion), kind=kCustom, calls=%fused_computation | custom fusion | bytes 2753856 | tf_op jit(solution)/shard_map/jit(_take)/gather | solution.py:40
  7.4 1.4 gather.7
  8.8 1.1 fusion.27
  9.9 30.0 %all_to_all.27 = bf16[48,7,128]{2,1,0:T(8,128)(2,1)S(1)} all-to-all(bf16[48,7,128]{2,1,0:T(8,128)(2,1)S(1)} %fusion.27), channel_id=1, replica_groups=mesh['ep'=48,'tp'=16] {'ep'}, dimensions={0} | all-to-all | bytes 172032 | tf_op jit(solution)/shard_map/all_to_all | solution.py:46
  40.0 0.2 broadcast_in_dim.54
  40.1 45.1 %all_to_all.28 = bf16[16,48,7,128]{3,1,2,0:T(8,128)(2,1)S(1)} all-to-all(bf16[16,48,7,128]{3,1,2,0:T(8,128)(2,1)S(1)} %broadcast_in_dim.54), channel_id=1, replica_groups=mesh['ep'=48,'tp'=16] {'tp'}, dimensions={0} | all-to-all | bytes 2752512 | tf_op jit(solution)/shard_map/all_to_all | solution.py:15
  85.2 0.0 copy-start.2
  85.2 0.4 copy.27
  85.6 0.9 copy-done.2
  86.4 0.0 copy-start.3
  86.4 1.3 fusion.3
  87.7 0.0 copy-done
  87.7 0.0 copy-done.3
  87.7 3.7 %fusion = bf16[42,16,8,128]{3,2,1,0:T(8,128)(2,1)} fusion(bf16[1,256,2048]{2,1,0:T(8,128)(2,1)S(1)} %copy-done, bf16[42,8,16,128]{3,2,1,0:T(8,128)(2,1)S(1)} %bitcast.48, bf16[1,2048,256]{2,1,0:T(8,128)(2,1)S(1)} %copy-done.3, f32[336,256]{1,0:T(8,128)} %fusion.3), kind=kOutput, calls=%fused_computation.2 | convolution fusion | flops 705847296 | bytes 5193728 | tf_op jit(solution)/shard_map/fd,rf->dr/dot_general | solution.py:54
  91.4 2.7 %copy.55 = bf16[42,16,8,128]{3,2,0,1:T(8,128)(2,1)} copy(bf16[42,16,8,128]{3,2,1,0:T(8,128)(2,1)} %fusion) | data formatting | bytes 2752512 | tf_op jit(solution)/shard_map/reshape | solution.py:24
  94.0 3.6 %all-to-all-start.2 = ((bf16[16,128,336]{1,2,0:T(8,128)(2,1)}), bf16[16,128,336]{1,2,0:T(8,128)(2,1)S(1)}, u32[]{:S(2)}, u32[]{:S(2)}) async-start(bf16[16,128,336]{1,2,0:T(8,128)(2,1)} %bitcast.45), calls=%async_computation.2 | async-start | bytes 2752512 | tf_op jit(solution)/shard_map/all_to_all | solution.py:29
  97.6 0.0 copy-start.1
  97.7 0.1 squeeze.19
  97.8 33.7 %all-to-all-done.2 = bf16[16,128,336]{1,2,0:T(8,128)(2,1)S(1)} async-done(((bf16[16,128,336]{1,2,0:T(8,128)(2,1)}), bf16[16,128,336]{1,2,0:T(8,128)(2,1)S(1)}, u32[]{:S(2)}, u32[]{:S(2)}) %all-to-all-start.2) | async-done | bytes 1376288 | tf_op jit(solution)/shard_map/all_to_all | solution.py:29
  131.5 0.2 reduce_sum.12
  131.7 0.7 all_to_all.20
  132.4 4.5 %all-to-all-start.3 = ((bf16[128,48,7]{0,2,1:T(8,128)(2,1)}), bf16[128,48,7]{0,2,1:T(8,128)(2,1)S(1)}, u32[]{:S(2)}, u32[]{:S(2)}) async-start(bf16[128,48,7]{0,2,1:T(8,128)(2,1)} %all_to_all.20), calls=%async_computation.3 | async-start | bytes 196608 | tf_op jit(solution)/shard_map/all_to_all | solution.py:60
  136.9 0.0 copy-done.1
  136.9 0.1 copy.22
  137.0 0.1 squeeze.20
  137.1 12.4 %all-to-all-done.3 = bf16[128,48,7]{0,2,1:T(8,128)(2,1)S(1)} async-done(((bf16[128,48,7]{0,2,1:T(8,128)(2,1)}), bf16[128,48,7]{0,2,1:T(8,128)(2,1)S(1)}, u32[]{:S(2)}, u32[]{:S(2)}) %all-to-all-start.3) | async-done | bytes 86048 | tf_op jit(solution)/shard_map/all_to_all | solution.py:60
  149.6 0.8 convolution_convert_fusion.1
  (6 shorter events, 0.1 us)
Async XLA Ops:
  0.0 87.7 %copy-start = (bf16[1,256,2048]{2,1,0:T(8,128)(2,1)S(1)}, bf16[1,256,2048]{2,1,0:T(8,128)(2,1)}, u32[]{:S(2)}) copy-start(bf16[1,256,2048]{2,1,0:T(8,128)(2,1)} %param.11) | copy-start | bytes 3145732
  85.2 1.2 copy-start.2
  86.4 1.3 copy-start.3
  94.0 37.5 %all-to-all-start.2 = ((bf16[16,128,336]{1,2,0:T(8,128)(2,1)}), bf16[16,128,336]{1,2,0:T(8,128)(2,1)S(1)}, u32[]{:S(2)}, u32[]{:S(2)}) async-start(bf16[16,128,336]{1,2,0:T(8,128)(2,1)} %bitcast.45), calls=%async_computation.2 | async-start | bytes 2752512 | tf_op jit(solution)/shard_map/all_to_all | solution.py:29
  97.6 39.3 %copy-start.1 = (f32[1,48,7]{1,0,2:T(1,128)S(1)}, f32[1,48,7]{1,0,2:T(1,128)}, u32[]{:S(2)}) copy-start(f32[1,48,7]{1,0,2:T(1,128)} %param.8) | copy-start | bytes 4036
  132.4 17.2 %all-to-all-start.3 = ((bf16[128,48,7]{0,2,1:T(8,128)(2,1)}), bf16[128,48,7]{0,2,1:T(8,128)(2,1)S(1)}, u32[]{:S(2)}, u32[]{:S(2)}) async-start(bf16[128,48,7]{0,2,1:T(8,128)(2,1)} %all_to_all.20), calls=%async_computation.3 | async-start | bytes 196608 | tf_op jit(solution)/shard_map/all_to_all | solution.py:60
where the time goes:
time: 151 us; the launch traced here: 150 us
  blocking collectives  75.1 us (50%)
  waiting for transfers between devices  46.2 us (31%)
  local copies, waits for them, and re-layouts  13.1 us (9%)
  starting transfers between devices  8.1 us (5%)
  matrix products  5.78 us (4%)
  other arithmetic  2.07 us (1%)
    all_to_all x1, blocking collectives, copy_for_each(): lax.all_to_all(jnp.broadcast_to(x[None], (count, *x.shape)), axis, 0, 0,...  45.1 us
    all_to_all x1, waiting for transfers between devices, summed_on_arrival(): parts = lax.all_to_all(in_blocks(x, dim, count), axis, 0, 0, tiled=True)  33.7 us
    all_to_all x1, blocking collectives, on_device(): lax.all_to_all(col_slice, 'ep', split_axis=0, concat_axis=0, tiled=True)  30 us
    all_to_all x1, waiting for transfers between devices, on_device(): lax.all_to_all(summed, 'ep', split_axis=1, concat_axis=1, tiled=True)  12.4 us
    gather x2, local copies, waits for them, and re-layouts, on_device(): picked = jnp.take(tokens, safe_ids, axis=0)  6.91 us
    all_to_all x1, starting transfers between devices, on_device(): lax.all_to_all(summed, 'ep', split_axis=1, concat_axis=1, tiled=True)  4.5 us
    dot_general x1, matrix products, on_device(): jnp.einsum('fd,rf->dr', down_local, hidden, preferred_element_type=jnp.fl...  3.68 us
    all_to_all x1, starting transfers between devices, summed_on_arrival(): parts = lax.all_to_all(in_blocks(x, dim, count), axis, 0, 0, tiled=True)  3.6 us
  transfers between devices with their start and end apart: 2, of which 2 were waited for; matrix products, arithmetic and copies ran while one was open for 0% of the time, Pallas kernels for 0%

commit v1 on v0

v1 whole, which is shorter than its diff:
```python
import functools

import jax
import jax.numpy as jnp
from jax import lax
from jax.experimental import pallas as pl
from jax.experimental.pallas import tpu as pltpu
from jax.sharding import PartitionSpec as P

MESH = pl.DeviceIdType.MESH
F32 = jnp.float32
BF16 = jnp.bfloat16
LANES = 128
PAD = 8


def dot(a, b, dims=((1,), (0,))):
    return lax.dot_general(a, b, (dims, ((), ())), preferred_element_type=F32)


def iota(shape, dim):
    return lax.broadcasted_iota(jnp.int32, shape, dim)


def kernel(
    experts, x_size, y_size, cap, slots,
    tokens_ref, chosen_ref, pick_ref, gate_ref, up_ref, down_ref, out_ref,
    tok_v, pad_v, wgu, wd_own, wd_peer, low, sel_hi, sel_lo, spread,
    sbuf, rbuf, sbuf2, rbuf2, xo, xp, acc, hid_own, hid_peer, part, rs_out, rs_in, ysum,
    tok_sem, wgu_sem, wd_sem, wdp_send, wdp_recv, a1_send, a1_recv, a2_send, a2_recv,
    ag_send, ag_recv, dd_send, dd_recv, hid_send, hid_recv, rs_send, rs_recv,
):
    ep = lax.axis_index("ep")
    tp = lax.axis_index("tp")
    z_size = experts // x_size
    z, x = lax.div(ep, x_size), lax.rem(ep, x_size)
    y, core = lax.div(tp, 2), lax.rem(tp, 2)
    rows = experts * PAD
    half = cap // 2 // 16 * 16
    half = cap - half if cap - half <= LANES else half
    spans = ((0, half), (half, cap - half))
    ffd = gate_ref.shape[2]
    depth = tokens_ref.shape[0]

    def chip(rel):
        return lax.rem(y + rel + y_size, y_size)

    def far_first(i, size):
        return size // 2 + ((i + 1) // 2) * (1 - 2 * (i % 2))

    def ep_peer(i):
        dz = far_first(lax.div(i, x_size), z_size)
        dx = far_first(lax.rem(i, x_size), x_size)
        return lax.rem(z + dz, z_size) * x_size + lax.rem(x + dx, x_size)

    peer = (ep, tp + 1 - 2 * core)
    ring = {1: (ep, chip(1) * 2 + core), -1: (ep, chip(-1) * 2 + core)}

    barrier = pltpu.get_barrier_semaphore()

    def greet(i, carry):
        pl.semaphore_signal(barrier, inc=1, device_id=(ep_peer(i), tp), device_id_type=MESH)
        return carry

    lax.fori_loop(0, experts - 1, greet, 0)
    for other in (peer, ring[1], ring[-1]):
        pl.semaphore_signal(barrier, inc=1, device_id=other, device_id_type=MESH)

    tok_copy = pltpu.make_async_copy(
        tokens_ref.at[:, pl.ds(pl.multiple_of(tp * LANES, LANES), LANES)], tok_v, tok_sem
    )
    tok_copy.start()
    order = [0]
    for k in range(1, y_size // 2):
        order += [-k, k]
    order.append(y_size // 2)
    slot_of = {rel: j for j, rel in enumerate(order)}
    slot_of[-(y_size // 2)] = slot_of[y_size // 2]
    for j, rel in enumerate(order):
        for side in range(2):
            lane_block = chip(rel) * 2 + (core if side == 0 else 1 - core)
            src = pl.ds(pl.multiple_of(lane_block * LANES, LANES), LANES)
            dst = pl.ds(j * 2 * LANES + side * LANES, LANES)
            for n, w_ref in enumerate((gate_ref, up_ref)):
                pltpu.make_async_copy(
                    w_ref.at[0, src, :], wgu.at[dst, pl.ds(n * ffd, ffd)], wgu_sem
                ).start()
    back = order[::-1]
    for j, rel in enumerate(back):
        cols = pl.ds(pl.multiple_of((chip(rel) * 2 + core) * LANES, LANES), LANES)
        pltpu.make_async_copy(
            down_ref.at[0, :, cols], wd_own.at[:, pl.ds(j * LANES, LANES)], wd_sem
        ).start()

    pad_v[0] = jnp.full((experts, LANES), -1.0, F32)
    pad_v[1] = jnp.zeros((experts, LANES), F32)
    pad_v[0, :, 0:slots] = chosen_ref[0].astype(F32)
    pad_v[1, :, 0:slots] = pick_ref[0]
    row_expert = (iota((rows, experts), 0) // PAD == iota((rows, experts), 1)).astype(BF16)
    row_slot = iota((rows, LANES), 0) % PAD
    lane = iota((rows, LANES), 1)
    ones = jnp.ones((LANES, LANES), BF16)
    mine = row_slot == lane
    named = dot(row_expert, pad_v[0].astype(BF16))
    token_of = dot(jnp.where(mine, named, 0.0).astype(BF16), ones)
    count = dot((named >= 0.0).astype(F32).astype(BF16), ones)
    chosen_here = (token_of.astype(jnp.int32) == lane) & (row_slot < slots)
    pick_one = jnp.where(chosen_here, 1.0, 0.0)
    tok_copy.wait()
    message = dot(pick_one.astype(BF16), tok_v[...])
    message = jnp.where(row_slot == PAD - 1, count, message)
    sbuf[...] = message.reshape(experts, PAD, LANES).astype(BF16)
    rbuf[ep] = sbuf[ep]

    pl.semaphore_wait(barrier, experts - 1 + 3)

    def exchange(src, dst, send_sem, recv_sem):
        def send(i, carry):
            other = ep_peer(i)
            pltpu.make_async_remote_copy(
                src_ref=src.at[other], dst_ref=dst.at[ep], send_sem=send_sem, recv_sem=recv_sem,
                device_id=(other, tp), device_id_type=MESH,
            ).start()
            return carry

        lax.fori_loop(0, experts - 1, send, 0)

    def exchanged(ref, sem):
        some = ref.at[pl.ds(0, experts - 1)]
        pltpu.make_async_copy(some, some, sem).wait()

    exchange(sbuf, rbuf, a1_send, a1_recv)

    for j, rel in enumerate(back):
        cols = pl.ds(pl.multiple_of((chip(rel) * 2 + 1 - core) * LANES, LANES), LANES)
        pltpu.make_async_remote_copy(
            src_ref=down_ref.at[0, :, cols], dst_ref=wd_peer.at[:, pl.ds(j * LANES, LANES)],
            send_sem=wdp_send, recv_sem=wdp_recv, device_id=peer, device_id_type=MESH,
        ).start()

    from_row = iota((rows, rows), 0)
    to_row = iota((rows, rows), 1)
    counts_row = from_row % PAD == PAD - 1
    low[:, 0:rows] = (counts_row & (from_row // PAD < to_row // PAD)).astype(F32).astype(BF16)
    low[:, rows : 2 * rows] = (
        counts_row & (from_row // PAD <= to_row // PAD)
    ).astype(F32).astype(BF16)
    weight = pad_v[1]
    weight_hi = weight.astype(BF16)
    weight_lo = (weight - weight_hi.astype(F32)).astype(BF16)
    for table, piece in ((sel_hi, weight_hi), (sel_lo, weight_lo)):
        spread_out = jnp.where(mine, dot(row_expert, piece), 0.0).astype(BF16)
        table[...] = jnp.transpose(dot(spread_out, ones) * pick_one).astype(BF16)
    acc[...] = jnp.zeros_like(acc)
    ysum[...] = jnp.zeros_like(ysum)

    exchanged(rbuf, a1_recv)
    arrived = rbuf[...].astype(F32).reshape(rows, LANES).astype(BF16)
    bounds = dot(arrived, low[...], ((0,), (0,)))
    first, end = bounds[:, 0:rows].astype(jnp.int32), bounds[:, rows : 2 * rows].astype(jnp.int32)
    slot_row = iota((LANES, rows), 1) % PAD
    places = []

    def ag_copy(sign, part_id, k):
        lo, size = spans[part_id]
        window = pl.ds(lo, size)
        index = ((0 if sign > 0 else 1) * 2 + part_id) * (y_size // 2) + k - 1
        return pltpu.make_async_remote_copy(
            src_ref=xo.at[slot_of[-sign * (k - 1)], window, :],
            dst_ref=xo.at[slot_of[-sign * k], window, :],
            send_sem=ag_send.at[index], recv_sem=ag_recv.at[index],
            device_id=ring[sign], device_id_type=MESH,
        )

    def dd_copy(j, part_id):
        lo, size = spans[part_id]
        window = pl.ds(lo, size)
        return pltpu.make_async_remote_copy(
            src_ref=xo.at[j, window, :], dst_ref=xp.at[j, window, :],
            send_sem=dd_send.at[j * 2 + part_id], recv_sem=dd_recv.at[j * 2 + part_id],
            device_id=peer, device_id_type=MESH,
        )

    last = {(1, 0): y_size // 2, (1, 1): y_size // 2 - 1, (-1, 1): y_size // 2, (-1, 0): y_size // 2 - 1}
    started = []

    def go(copy):
        copy.start()
        started.append(copy)

    for part_id, (lo, size) in enumerate(spans):
        base = iota((LANES, rows), 0) + lo
        here = (first + slot_row == base) & (base < end)
        if size < LANES:
            here = here & (base < lo + size)
        place = jnp.where(here, 1.0, 0.0)
        places.append(place)
        xo[0, lo : lo + size, :] = dot(place.astype(BF16), arrived)[0:size].astype(BF16)
        for sign in (1, -1):
            go(ag_copy(sign, part_id, 1))
        go(dd_copy(0, part_id))
    for part_id, (lo, size) in enumerate(spans):
        spread[part_id] = jnp.transpose(places[part_id]).astype(BF16)

    pltpu.make_async_copy(wgu, wgu, wgu_sem).wait()

    def multiply(rel):
        j = slot_of[rel]
        for part_id in range(2):
            dd_copy(j, part_id).wait_recv()
        lhs = jnp.concatenate([xo[j], xp[j]], axis=1)
        acc[...] += dot(lhs, wgu[j * 2 * LANES : (j + 1) * 2 * LANES, :])

    for k in range(1, y_size // 2 + 1):
        if k == 1:
            multiply(0)
        for sign, part_id in ((1, 0), (-1, 1), (1, 1), (-1, 0)):
            if k > last[sign, part_id]:
                continue
            ag_copy(sign, part_id, k).wait_recv()
            if k < last[sign, part_id]:
                go(ag_copy(sign, part_id, k + 1))
            go(dd_copy(slot_of[-sign * k], part_id))
        if k > 1:
            multiply(-(k - 1))
            multiply(k - 1)
    multiply(y_size // 2)

    gate, up = acc[:, 0:ffd], acc[:, ffd : 2 * ffd]
    hid_own[...] = (gate / (1.0 + jnp.exp(-gate)) * up).astype(BF16)
    hid_copy = pltpu.make_async_remote_copy(
        src_ref=hid_own, dst_ref=hid_peer, send_sem=hid_send, recv_sem=hid_recv,
        device_id=peer, device_id_type=MESH,
    )
    go(hid_copy)
    pltpu.make_async_copy(wd_own, wd_own, wd_sem).wait()
    part[...] = dot(hid_own[...], wd_own[...])
    pltpu.make_async_copy(wd_peer, wd_peer, wdp_recv).wait()
    hid_copy.wait_recv()

    block_of = {rel: j for j, rel in enumerate(back)}
    block_of[-(y_size // 2)] = 0

    def rs_index(sign, part_id, k):
        return ((0 if sign > 0 else 1) * 2 + part_id) * (y_size // 2) + k - 1

    def rs_copy(sign, part_id, k):
        index = rs_index(sign, part_id, k)
        window = pl.ds(0, spans[part_id][1])
        return pltpu.make_async_remote_copy(
            src_ref=rs_out.at[index, window, :], dst_ref=rs_in.at[index, window, :],
            send_sem=rs_send.at[index], recv_sem=rs_recv.at[index],
            device_id=ring[sign], device_id_type=MESH,
        )

    def own(rel, part_id):
        lo, size = spans[part_id]
        j = block_of[rel]
        return part[lo : lo + size, j * LANES : (j + 1) * LANES]

    def rs_step(sign, part_id, k):
        rel = sign * (last[sign, part_id] + 1 - k)
        total = own(rel, part_id)
        size = spans[part_id][1]
        if k > 1:
            rs_copy(sign, part_id, k - 1).wait_recv()
            total += rs_in[rs_index(sign, part_id, k - 1), 0:size, :].astype(F32)
        rs_out[rs_index(sign, part_id, k), 0:size, :] = total.astype(BF16)
        go(rs_copy(sign, part_id, k))

    def add_peer(j, count):
        cols = slice(j * LANES, (j + count) * LANES)
        part[:, cols] += dot(hid_peer[...], wd_peer[:, cols])

    add_peer(0, 1)
    rs_step(1, 0, 1)
    rs_step(-1, 1, 1)
    add_peer(1, 2)
    rs_step(1, 1, 1)
    rs_step(-1, 0, 1)
    add_peer(3, y_size - 3)
    for k in range(2, y_size // 2 + 1):
        for sign, part_id in ((1, 0), (-1, 1), (1, 1), (-1, 0)):
            if k <= last[sign, part_id]:
                rs_step(sign, part_id, k)
    for part_id, (lo, size) in enumerate(spans):
        total = own(0, part_id)
        for sign in (1, -1) if part_id == 1 else (-1, 1):
            k = last[sign, part_id]
            rs_copy(sign, part_id, k).wait_recv()
            total += rs_in[rs_index(sign, part_id, k), 0:size, :].astype(F32)
        ysum[part_id, 0:size, :] = total.astype(BF16)

    result = dot(spread[0], ysum[0]) + dot(spread[1], ysum[1])
    sbuf2[...] = result.reshape(experts, PAD, LANES).astype(BF16)
    exchange(sbuf2, rbuf2, a2_send, a2_recv)
    rbuf2[ep] = sbuf2[ep]
    exchanged(rbuf2, a2_recv)
    got = rbuf2[...].astype(F32).reshape(rows, LANES).astype(BF16)
    out_ref[...] = (dot(sel_hi[...], got) + dot(sel_lo[...], got)).astype(out_ref.dtype)

    for copy in started:
        copy.wait_send()
    exchanged(sbuf, a1_send)
    exchanged(sbuf2, a2_send)
    pltpu.make_async_copy(wd_peer, wd_peer, wdp_send).wait()


def on_device(experts, x_size, y_size, cap, tokens, chosen, pick_weight, gate_weight, up_weight, down_weight):
    depth, width = tokens.shape
    slots = chosen.shape[2]
    ffd = gate_weight.shape[2]
    rows = experts * PAD
    messages = 4 * (y_size // 2)
    dma = pltpu.SemaphoreType.DMA
    hbm = pl.BlockSpec(memory_space=pltpu.MemorySpace.HBM)
    vmem = pl.BlockSpec(memory_space=pltpu.MemorySpace.VMEM)
    return pl.pallas_call(
        functools.partial(kernel, experts, x_size, y_size, cap, slots),
        out_shape=jax.ShapeDtypeStruct((depth, LANES), BF16),
        in_specs=[hbm, vmem, vmem, hbm, hbm, hbm],
        out_specs=vmem,
        scratch_shapes=[
            pltpu.VMEM((depth, LANES), BF16),
            pltpu.VMEM((2, experts, LANES), F32),
            pltpu.VMEM((width, 2 * ffd), BF16),
            pltpu.VMEM((ffd, y_size * LANES), BF16),
            pltpu.VMEM((ffd, y_size * LANES), BF16),
            pltpu.VMEM((rows, 2 * rows), BF16),
            pltpu.VMEM((depth, rows), BF16),
            pltpu.VMEM((depth, rows), BF16),
            pltpu.VMEM((2, rows, LANES), BF16),
            pltpu.VMEM((experts, PAD, LANES), BF16),
            pltpu.VMEM((experts, PAD, LANES), BF16),
            pltpu.VMEM((experts, PAD, LANES), BF16),
            pltpu.VMEM((experts, PAD, LANES), BF16),
            pltpu.VMEM((y_size, cap, LANES), BF16),
            pltpu.VMEM((y_size, cap, LANES), BF16),
            pltpu.VMEM((cap, 2 * ffd), F32),
            pltpu.VMEM((cap, ffd), BF16),
            pltpu.VMEM((cap, ffd), BF16),
            pltpu.VMEM((cap, y_size * LANES), F32),
            pltpu.VMEM((messages, LANES, LANES), BF16),
            pltpu.VMEM((messages, LANES, LANES), BF16),
            pltpu.VMEM((2, LANES, LANES), BF16),
            dma, dma, dma, dma, dma, dma, dma, dma, dma,
            dma((messages,)), dma((messages,)),
            dma((2 * y_size,)), dma((2 * y_size,)),
            dma, dma,
            dma((messages,)), dma((messages,)),
        ],
        compiler_params=pltpu.CompilerParams(collective_id=0, has_side_effects=True),
        name="experts",
    )(tokens, chosen, pick_weight, gate_weight, up_weight, down_weight)


def solution(mesh, x_size=4, cap=240):
    experts, tp = mesh.shape["ep"], mesh.shape["tp"]
    return jax.shard_map(
        functools.partial(on_device, experts, x_size, tp // 2, cap),
        mesh=mesh,
        in_specs=(
            P("ep", None),
            P("ep", None, None),
            P("ep", None, None),
            P("ep", None, "tp"),
            P("ep", None, "tp"),
            P("ep", "tp", None),
        ),
        out_specs=P("ep", "tp"),
        check_vma=False,
    )
```

time: 151 us -> 68.9 us (0.46)
  the two profiles are of different devices: /device:TPU:1 before, /device:TPU:8 now
where the time goes in v1:
time: 68.9 us; the launch traced here: 68.5 us
  Pallas kernels  65.1 us (94%)
  local copies, waits for them, and re-layouts  3.47 us (5%)
    pallas_call x1, Pallas kernels, on_device(): pl.pallas_call(functools.partial(kernel, experts, x_size, y_size, cap, sl...  65.1 us
    unnamed x5, local copies, waits for them, and re-layouts  3.47 us

profile of v1, /device:TPU:8, one launch (start us, length us, event | category | flops | bytes accessed | tf_op | source)
XLA Modules:
  0.0 68.5 jit_solution(8570542430318905367)
XLA Ops:
  0.0 0.0 copy-start
  0.0 1.4 %copy.7.chosen_ref = s32[1,48,7]{2,1,0:T(8,128)} copy(s32[1,48,7]{1,0,2:T(1,128)} %param.7) | data formatting | bytes 2688 | tf_op args[1]
  1.4 0.0 copy-done
  1.4 0.7 %copy.8.pick_ref = f32[1,48,7]{2,1,0:T(8,128)} copy(f32[1,48,7]{1,0,2:T(1,128)S(1)} %copy-done) | data formatting | bytes 2688 | tf_op args[2]
  2.1 65.1 %experts.1 = bf16[128,128]{1,0:T(8,128)(2,1)} custom-call(bf16[128,2048]{1,0:T(8,128)(2,1)} %tokens_ref.1, s32[1,48,7]{2,1,0:T(8,128)} %copy.7.chosen_ref, f32[1,48,7]{2,1,0:T(8,128)} %copy.8.pick_ref, bf16[1,2048,256]{2,1,0:T(8,128)(2,1)} %gate_ref.1, bf16[1,2048,256]{2,1,0:T(8,128)(2,1)} %up_ref.1, bf16[1,256,2048]{2,1,0:T(8,128)(2,1)} %down_ref.1), custom_call_target="tpu_custom_call" | custom-call | tf_op jit(solution)/shard_map/experts/pallas_call | solution.py:318
  67.2 1.4 %copy.10 = bf16[128,128]{1,0:T(8,128)(2,1)} copy(bf16[128,128]{1,0:T(8,128)(2,1)} %experts.1) | data formatting | bytes 65536
Async XLA Ops:
  0.0 1.4 %copy-start = (f32[1,48,7]{1,0,2:T(1,128)S(1)}, f32[1,48,7]{1,0,2:T(1,128)}, u32[]{:S(2)}) copy-start(f32[1,48,7]{1,0,2:T(1,128)} %param.8) | copy-start | bytes 4036
